TPU v7x, 128 devices: a whole 4x4x4 slice. The times are simulated.
128 devices in a mesh: ep: 128 (over z, y, x, core).
Axes of the slice: x: 4, y: 4, z: 4, core: 2. Of those that a mesh axis runs over, the one named last changes fastest.
Arguments:
- tokens: bfloat16 [512, 2048], P('ep'), may hold values from -6 to 6
- lengths: int32 [512], P('ep'), may hold values from 1 to 1023
- cache_keys: bfloat16 [512, 1024, 2, 128], P('ep')
- cache_values: bfloat16 [512, 1024, 2, 128], P('ep'), may hold values from -6 to 6
- query_w: bfloat16 [2048, 1024], replicated, may hold values from -0.125 to 0.125
- key_w: bfloat16 [2048, 256], replicated, may hold values from -0.125 to 0.125
- value_w: bfloat16 [2048, 256], replicated, may hold values from -0.125 to 0.125
- out_w: bfloat16 [1024, 2048], replicated, may hold values from -0.1875 to 0.1875
- mix_lambda: float32 [8], replicated, may hold values from 0.3 to 0.8
- head_gain: float32 [128], replicated, may hold values from 0.1 to 1.9
- attn_gain: float32 [2048], replicated, may hold values from 0.1 to 1.9
- ffn_gain: float32 [2048], replicated, may hold values from 0.1 to 1.9
- routes: int32 [512, 2], P('ep'), may hold values from 0 to 7, all different within a row; in each aligned block of 4 rows (0 to 3, 4 to 7, ...) at most 2 rows name the same one
- route_weights: float32 [512, 2], P('ep'), may hold values from 0.2 to 1
- exp_gate: bfloat16 [2048, 49152], P(None, 'ep'), may hold values from -0.125 to 0.125
- exp_up: bfloat16 [2048, 49152], P(None, 'ep'), may hold values from -0.125 to 0.125
- exp_down: bfloat16 [49152, 2048], P('ep'), may hold values from -0.078125 to 0.078125
- dense_gate: bfloat16 [128, 256, 352], P('ep'), may hold values from -0.125 to 0.125
- dense_up: bfloat16 [128, 256, 352], P('ep'), may hold values from -0.125 to 0.125
- dense_down: bfloat16 [128, 352, 256], P('ep'), may hold values from -0.078125 to 0.078125
- branch_gate: bfloat16 [2048], replicated, may hold values from -0.125 to 0.125
Outputs:
- output: bfloat16 [512, 2048], P('ep')
- new_keys: bfloat16 [512, 256], P('ep')
- new_values: bfloat16 [512, 256], P('ep')
Inputs may be any that keep to these rules, and one draw needn't show every extreme that they name: `routes`: each row names 2 different experts; among the 4 rows of one device no expert is named by more than 2 rows, a bound that some block reaches.
All inputs are finite; a program needn't handle non-finite values.
Results may differ from a plain program's by a relative error of at most 0.015.
Values may be sent and summed in bfloat16 or wider, within the bound.
A program may use at most 128 MiB of HBM per device.

v0:
```python
import jax
import jax.numpy as jnp
from jax import lax
from jax.sharding import PartitionSpec as P

HEADS = 8
KV_HEADS = 2
HEAD_DIM = 128
SEQ_DEV = 4
TOP_K = 2
SPLIT = 16


def sent_together(arrays, axis, split_dim, concat_dim, along):
    widths = [a.shape[along] for a in arrays]
    both = jnp.concatenate(arrays, axis=along)
    filled = lax.all_to_all(both, axis, split_axis=split_dim, concat_axis=concat_dim, tiled=True)
    return tuple(jnp.split(filled, [sum(widths[:k]) for k in range(1, len(widths))], axis=along))


def split_up(x, dim, peers):
    before, after = (x.shape[:dim], x.shape[dim + 1 :])
    return jnp.moveaxis(x.reshape(*before, peers, -1, *after), dim, 0)


def cut_rows(length, count):
    unit = 8 if length >= 8 * count else 1
    return [length // unit * k // count * unit for k in range(1, count)]


def in_order(tiles, dim):
    lengths = list(tiles.shape[1:])
    lengths[dim] *= tiles.shape[0]
    return jnp.moveaxis(tiles, 0, dim).reshape(lengths)


def exchange_in_pieces(x, axis, pieces, split_dim, concat_dim):
    tiles = split_up(x, split_dim, lax.axis_size(axis))
    cut = max(range(1, max(2, tiles.ndim - 1)), key=lambda d: tiles.shape[d])
    outs = []
    for piece in jnp.split(tiles, cut_rows(tiles.shape[cut], pieces), axis=cut):
        if piece.size:
            outs.append(lax.all_to_all(piece, axis, split_axis=0, concat_axis=0, tiled=True))
    return in_order(jnp.concatenate(outs, axis=cut), concat_dim)


def rms_norm(values, gain, epsilon):
    scale = lax.rsqrt(jnp.mean(values * values, axis=-1, keepdims=True) + epsilon)
    return values * scale * gain


def softmax_pair(scores, own_score, valid):
    masked = jnp.where(valid, scores, -jnp.inf)
    largest = jnp.maximum(jnp.max(masked, axis=-1), own_score)
    raised = jnp.where(valid, jnp.exp(scores - largest[..., None]), 0.0)
    own_raised = jnp.exp(own_score - largest)
    total = jnp.sum(raised, axis=-1) + own_raised
    return (raised / total[..., None], own_raised / total)


def swiglu_rows(chosen, w_gate, w_up, w_down):
    gate_part = jnp.dot(chosen, w_gate, preferred_element_type=jnp.float32)
    up_part = jnp.dot(chosen, w_up, preferred_element_type=jnp.float32)
    act = (jax.nn.silu(gate_part) * up_part).astype(jnp.bfloat16)
    return jnp.dot(act, w_down, preferred_element_type=jnp.float32)


def per_device(
    tokens,
    lengths,
    cache_keys,
    cache_values,
    query_w,
    key_w,
    value_w,
    out_w,
    mix_lambda,
    head_gain,
    attn_gain,
    ffn_gain,
    routes,
    route_weights,
    exp_gate,
    exp_up,
    exp_down,
    dense_gate,
    dense_up,
    dense_down,
    branch_gate,
):
    rows = tokens.shape[0]
    groups = HEADS // KV_HEADS
    half = HEAD_DIM // 2
    scale = (HEAD_DIM // 2) ** (-0.5)
    cache_len = cache_keys.shape[1]
    xfull = tokens.astype(jnp.float32)
    normed = rms_norm(xfull, attn_gain, 1e-06).astype(jnp.bfloat16)
    query = jnp.dot(normed, query_w, preferred_element_type=jnp.float32).astype(jnp.bfloat16)
    key_new = jnp.dot(normed, key_w, preferred_element_type=jnp.float32).astype(jnp.bfloat16)
    value_new = jnp.dot(normed, value_w, preferred_element_type=jnp.float32).astype(jnp.bfloat16)
    qheads = query.reshape(rows, KV_HEADS, groups, HEAD_DIM)
    knew = key_new.reshape(rows, KV_HEADS, HEAD_DIM)
    vnew = value_new.reshape(rows, KV_HEADS, HEAD_DIM)
    valid = (jnp.arange(cache_len, dtype=jnp.int32)[None, :] < lengths[:, None])[:, None, None, :]
    first = (
        jnp.einsum(
            "sgqd,spgd->sgqp",
            qheads[..., :half],
            cache_keys[..., :half],
            preferred_element_type=jnp.float32,
        )
        * scale
    )
    first_own = (
        jnp.einsum(
            "sgqd,sgd->sgq",
            qheads[..., :half],
            knew[..., :half],
            preferred_element_type=jnp.float32,
        )
        * scale
    )
    second = (
        jnp.einsum(
            "sgqd,spgd->sgqp",
            qheads[..., half:],
            cache_keys[..., half:],
            preferred_element_type=jnp.float32,
        )
        * scale
    )
    second_own = (
        jnp.einsum(
            "sgqd,sgd->sgq",
            qheads[..., half:],
            knew[..., half:],
            preferred_element_type=jnp.float32,
        )
        * scale
    )
    prob_one, own_one = softmax_pair(first, first_own, valid)
    prob_two, own_two = softmax_pair(second, second_own, valid)
    lam = mix_lambda.reshape(KV_HEADS, groups)
    weights = (prob_one - lam[None, :, :, None] * prob_two).astype(jnp.bfloat16)
    own_weights = (own_one - lam[None] * own_two).astype(jnp.bfloat16)
    mixed = jnp.einsum("sgqp,spgd->sgqd", weights, cache_values, preferred_element_type=jnp.float32)
    mixed = (
        mixed + own_weights.astype(jnp.float32)[..., None] * vnew.astype(jnp.float32)[:, :, None, :]
    )
    heads = rms_norm(mixed, head_gain, 1e-05).astype(jnp.bfloat16).reshape(rows, HEADS * HEAD_DIM)
    hidden_state = xfull + jnp.dot(heads, out_w, preferred_element_type=jnp.float32)
    ffn_in = rms_norm(hidden_state, ffn_gain, 1e-06).astype(jnp.bfloat16)
    devices = lax.axis_size("ep")
    experts = devices // SPLIT
    row_blocks = devices // SPLIT
    capacity = min(SEQ_DEV, max(2, SEQ_DEV * TOP_K * 2 // experts))
    slots = jnp.arange(capacity, dtype=jnp.int32)
    all_rows = lax.all_gather(ffn_in, "ep", axis=0, tiled=True)
    gate = jax.nn.sigmoid(jnp.dot(ffn_in, branch_gate, preferred_element_type=jnp.float32))
    position = lax.axis_index("ep")
    row_span = dense_gate.shape[1]
    col_span = dense_gate.shape[2]
    row_block = position // SPLIT
    columns = lax.dynamic_slice_in_dim(all_rows, row_block * row_span, row_span, 1)
    gate_tile = jnp.dot(columns, dense_gate[0], preferred_element_type=jnp.float32).reshape(
        devices, rows, col_span
    )
    up_tile = jnp.dot(columns, dense_up[0], preferred_element_type=jnp.float32).reshape(
        devices, rows, col_span
    )
    gate_in, up_in = tuple(
        (
            part.astype(jnp.float32)
            for part in sent_together(
                (gate_tile.astype(jnp.bfloat16), up_tile.astype(jnp.bfloat16)), "ep", 0, 0, 1
            )
        )
    )
    gate_sum = jnp.sum(gate_in.reshape(row_blocks, SPLIT, rows, col_span), axis=0)
    up_sum = jnp.sum(up_in.reshape(row_blocks, SPLIT, rows, col_span), axis=0)
    own_act = (jax.nn.silu(gate_sum) * up_sum).astype(jnp.bfloat16)
    outgoing_act = jnp.tile(own_act, (row_blocks, 1, 1))
    act_in = lax.all_to_all(outgoing_act, "ep", split_axis=0, concat_axis=0, tiled=True)
    down_tile = jnp.dot(
        act_in.reshape(devices * rows, col_span), dense_down[0], preferred_element_type=jnp.float32
    )
    down_in = lax.all_to_all(
        down_tile.reshape(devices, rows, row_span).astype(jnp.bfloat16),
        "ep",
        split_axis=0,
        concat_axis=0,
        tiled=True,
    ).astype(jnp.float32)
    down_sum = jnp.sum(down_in.reshape(row_blocks, SPLIT, rows, row_span), axis=1)
    dense = jnp.transpose(down_sum, (1, 0, 2)).reshape(rows, row_blocks * row_span)
    expert_ids = jnp.arange(experts, dtype=jnp.int32)
    match = routes[None, :, :] == expert_ids[:, None, None]
    weight = jnp.sum(jnp.where(match, route_weights[None], 0.0), axis=-1)
    hit = jnp.any(match, axis=-1).astype(jnp.int32)
    rank = jnp.cumsum(hit, axis=1) - 1
    select = (hit[:, None, :] == 1) & (rank[:, None, :] == slots[None, :, None])
    chosen = jnp.einsum(
        "ecs,sd->ecd", select.astype(jnp.bfloat16), ffn_in, preferred_element_type=jnp.float32
    ).astype(jnp.bfloat16)
    outgoing = jnp.repeat(chosen, SPLIT, axis=0)
    incoming = lax.all_to_all(outgoing, "ep", split_axis=0, concat_axis=0, tiled=True)
    sources = incoming.shape[0]
    taken = incoming.shape[1]
    result = swiglu_rows(incoming.reshape(sources * taken, -1), exp_gate, exp_up, exp_down)
    returned = exchange_in_pieces(
        result.reshape(sources, taken, -1).astype(jnp.bfloat16), "ep", 2, 0, 0
    ).astype(jnp.float32)
    summed = jnp.sum(returned.reshape(experts, SPLIT, capacity, -1), axis=1)
    weighted = select.astype(jnp.float32) * weight[:, None, :]
    routed = jnp.einsum("ecs,ecd->sd", weighted, summed, precision=lax.Precision.HIGHEST)
    output = (hidden_state + routed + gate[:, None] * dense).astype(jnp.bfloat16)
    return (output, key_new, value_new)


def solution(mesh):
    placed = (
        P("ep", None),
        P("ep"),
        P("ep", None, None, None),
        P("ep", None, None, None),
        P(),
        P(),
        P(),
        P(),
        P(),
        P(),
        P(),
        P(),
        P("ep", None),
        P("ep", None),
        P(None, "ep"),
        P(None, "ep"),
        P("ep", None),
        P("ep", None, None),
        P("ep", None, None),
        P("ep", None, None),
        P(),
    )
    return jax.shard_map(
        per_device,
        mesh=mesh,
        in_specs=placed,
        out_specs=(P("ep", None), P("ep", None), P("ep", None)),
        check_vma=False,
    )
```

profile of v0, /device:TPU:1, one launch (start us, length us, event | category | flops | bytes accessed | tf_op | source)
XLA Modules:
  0.0 199.1 jit_solution(3395068889452520648)
XLA Ops:
  8.2 2.9 %convolution_convert_fusion.5 = bf16[4,1024]{1,0:T(4,128)(2,1)S(1)} fusion(bf16[2048,1024]{1,0:T(8,128)(2,1)} %param.25, bf16[4,2048]{1,0:T(4,128)(2,1)} %param.21, f32[2048]{0:T(1024)} %param.31, f32[4]{0:T(128)S(1)} %add_rsqrt_fusion.2), kind=kOutput, calls=%fused_computation.22 | convolution fusion | flops 16814080 | bytes 4227088 | tf_op jit(solution)/shard_map/dot_general | solution.py:98
  11.3 6.8 %fusion.79 = (bf16[4,1024,2,64]{3,2,1,0:T(2,128)(2,1)}, bf16[4,1024,2,64]{3,2,1,0:T(2,128)(2,1)}) fusion(bf16[4,1024,2,128]{3,2,1,0:T(2,128)(2,1)} %param.23), kind=kLoop, calls=%fused_computation.114 | loop fusion | bytes 4194304 | tf_op jit(solution)/shard_map/slice | solution.py:127
  19.2 2.5 %select_reduce_fusion.1 = (f32[4,2,4]{2,1,0:T(2,128)S(1)}, f32[4,2,4,1024]{3,2,1,0:T(4,128)S(1)}) fusion(pred[4,1024]{1,0:T(4,128)(4,1)S(1)} %iota_compare_fusion, bf16[4,1024,2,64]{3,2,1,0:T(2,128)(2,1)} %get-tuple-element.6, bf16[4,2,4,128]{3,2,1,0:T(4,128)(2,1)S(1)} %reshape.159), kind=kOutput, calls=%fused_computation.52 | convolution fusion | flops 4292576 | bytes 1192064 | tf_op jit(solution)/shard_map/sgqd,spgd->sgqp/dot_general | solution.py:106
  23.5 3.0 %multiply_reduce_fusion = (f32[4]{0:T(128)S(1)}, f32[4,2048]{1,0:T(4,128)S(1)}) fusion(bf16[4,1024]{1,0:T(4,128)(2,1)S(1)} %reshape.161, bf16[1024,2048]{1,0:T(8,128)(2,1)} %param.28, bf16[4,2048]{1,0:T(4,128)(2,1)S(1)} %copy-done.6), kind=kOutput, calls=%fused_computation.70 | convolution fusion | flops 16809980 | bytes 4251664 | tf_op jit(solution)/shard_map/dot_general | solution.py:151
  27.7 1.6 broadcast_in_dim.69
  29.3 12.0 %all-to-all-start = ((bf16[128,2,2048]{2,1,0:T(2,128)(2,1)}), bf16[128,2,2048]{2,1,0:T(2,128)(2,1)}, u32[]{:S(2)}, u32[]{:S(2)}) async-start(bf16[128,2,2048]{2,1,0:T(2,128)(2,1)} %bitcast.7), calls=%async_computation | async-start | bytes 2097152 | tf_op jit(solution)/shard_map/all_to_all | solution.py:206
  41.3 19.0 %all-to-all-done = bf16[128,2,2048]{2,1,0:T(2,128)(2,1)} async-done(((bf16[128,2,2048]{2,1,0:T(2,128)(2,1)}), bf16[128,2,2048]{2,1,0:T(2,128)(2,1)}, u32[]{:S(2)}, u32[]{:S(2)}) %all-to-all-start) | async-done | bytes 1048608 | tf_op jit(solution)/shard_map/all_to_all | solution.py:206
  60.4 1.5 reshape.163
  61.9 2.9 %fusion.82 = f32[256,384]{1,0:T(8,128)} fusion(bf16[256,2048]{1,0:T(8,128)(2,1)S(1)} %reshape.163, bf16[2048,384]{1,0:T(8,128)(2,1)} %param.35), kind=kOutput, calls=%fused_computation.117 | convolution fusion | flops 402653184 | bytes 3014656 | tf_op jit(solution)/shard_map/dot_general | solution.py:62
  64.7 4.4 %convolution_convert_fusion = bf16[256,2048]{1,0:T(8,128)(2,1)} fusion(bf16[384,2048]{1,0:T(8,128)(2,1)} %param.37, bf16[256,2048]{1,0:T(8,128)(2,1)S(1)} %reshape.163, bf16[2048,384]{1,0:T(8,128)(2,1)} %param.36, f32[256,384]{1,0:T(8,128)} %fusion.82), kind=kOutput, calls=%fused_computation | convolution fusion | flops 806420480 | bytes 5636096 | tf_op jit(solution)/shard_map/dot_general | solution.py:65
  69.1 1.7 convert_element_type.121
  70.8 2.5 %fusion.80 = (bf16[128,1,1,2048]{3,2,1,0:T(2,128)(2,1)}, bf16[128,1,1,2048]{3,2,1,0:T(2,128)(2,1)}) fusion(bf16[128,1,2,2048]{3,2,1,0:T(2,128)(2,1)S(1)} %bitcast.73), kind=kLoop, calls=%fused_computation.115 | loop fusion | bytes 2097152 | tf_op jit(solution)/shard_map/split | solution.py:41
  73.9 4.7 %reduce = bf16[128,2048]{1,0:T(8,128)(2,1)S(1)} reduce(bf16[128,1,1,2048]{3,2,1,0:T(2,128)(2,1)} %get-tuple-element.8, bf16[]{:T(256)} %broadcast.142), dimensions={1,2}, to_apply=%get-tuple-element.8.reduce_sub_computation | reduce | bytes 1048578 | tf_op jit(solution)/shard_map/split | solution.py:41
  79.8 5.4 %all-to-all-start.2 = ((bf16[128,2,1024]{2,1,0:T(2,128)(2,1)}), bf16[128,2,1024]{2,1,0:T(2,128)(2,1)}, u32[]{:S(2)}, u32[]{:S(2)}) async-start(bf16[128,2,1024]{2,1,0:T(2,128)(2,1)} %reshape.192), calls=%async_computation.2 | async-start | bytes 1048576 | tf_op jit(solution)/shard_map/all_to_all | solution.py:43
  85.2 19.9 %all-gather.3.cloned.1.call-done = bf16[128,4,2048]{2,1,0:T(4,128)(2,1)} async-done(((bf16[1,4,2048]{2,1,0:T(4,128)(2,1)}), bf16[128,4,2048]{2,1,0:T(4,128)(2,1)}) %all-gather.3.cloned.1.call-update) | async-done | bytes 2097168 | tf_op jit(solution)/shard_map/all_gather | solution.py:158
  105.1 4.0 %reshape.180 = bf16[512,2048]{1,0:T(8,128)(2,1)} reshape(bf16[128,4,2048]{2,1,0:T(4,128)(2,1)} %all-gather.3.cloned.1.call-done) | data formatting | bytes 4194304
  111.6 2.4 %copy.84 = bf16[128,8,352]{2,1,0:T(8,128)(2,1)} copy(bf16[128,8,352]{0,2,1:T(8,128)(2,1)} %pad_maximum_fusion.1) | data formatting | bytes 1441792 | tf_op jit(solution)/shard_map/concatenate | solution.py:16
  114.1 6.1 %all-to-all-start.3 = ((bf16[128,8,352]{2,1,0:T(8,128)(2,1)}), bf16[128,8,352]{2,1,0:T(8,128)(2,1)}, u32[]{:S(2)}, u32[]{:S(2)}) async-start(bf16[128,8,352]{2,1,0:T(8,128)(2,1)} %copy.84), calls=%async_computation.3 | async-start | bytes 1572864 | tf_op jit(solution)/shard_map/all_to_all | solution.py:17
  120.2 4.4 %reduce.1 = bf16[128,2048]{1,0:T(8,128)(2,1)} reduce(bf16[128,1,1,2048]{3,2,1,0:T(2,128)(2,1)S(1)} %copy-done.1, bf16[]{:T(256)} %broadcast.142), dimensions={1,2}, to_apply=%get-tuple-element.7.reduce_sub_computation | reduce | bytes 1048578 | tf_op jit(solution)/shard_map/split | solution.py:41
  124.6 2.2 %reshape.194 = bf16[128,2,1024]{2,1,0:T(2,128)(2,1)} reshape(bf16[128,2048]{1,0:T(8,128)(2,1)} %reduce.1) | data formatting | bytes 1048576
  126.8 9.4 %all-to-all-done.3 = bf16[128,8,352]{2,1,0:T(8,128)(2,1)} async-done(((bf16[128,8,352]{2,1,0:T(8,128)(2,1)}), bf16[128,8,352]{2,1,0:T(8,128)(2,1)}, u32[]{:S(2)}, u32[]{:S(2)}) %all-to-all-start.3) | async-done | bytes 720928 | tf_op jit(solution)/shard_map/all_to_all | solution.py:17
  136.3 4.5 %all-to-all-start.1 = ((bf16[128,2,1024]{2,1,0:T(2,128)(2,1)}), bf16[128,2,1024]{2,1,0:T(2,128)(2,1)S(1)}, u32[]{:S(2)}, u32[]{:S(2)}) async-start(bf16[128,2,1024]{2,1,0:T(2,128)(2,1)} %reshape.194), calls=%async_computation.1 | async-start | bytes 1048576 | tf_op jit(solution)/shard_map/all_to_all | solution.py:43
  140.8 1.7 fusion.81
  143.9 10.5 %all-to-all-done.1 = bf16[128,2,1024]{2,1,0:T(2,128)(2,1)S(1)} async-done(((bf16[128,2,1024]{2,1,0:T(2,128)(2,1)}), bf16[128,2,1024]{2,1,0:T(2,128)(2,1)S(1)}, u32[]{:S(2)}, u32[]{:S(2)}) %all-to-all-start.1) | async-done | bytes 524320 | tf_op jit(solution)/shard_map/all_to_all | solution.py:43
  154.4 5.4 %all-to-all-start.4 = ((bf16[128,4,352]{2,1,0:T(4,128)(2,1)}), bf16[128,4,352]{2,1,0:T(4,128)(2,1)}, u32[]{:S(2)}, u32[]{:S(2)}) async-start(bf16[128,4,352]{2,1,0:T(4,128)(2,1)} %copy.87), calls=%async_computation.4 | async-start | bytes 786432 | tf_op jit(solution)/shard_map/all_to_all | solution.py:183
  160.0 3.6 %reshape.193 = bf16[128,1,1,2048]{3,2,1,0:T(2,128)(2,1)S(1)} reshape(bf16[128,2,1024]{2,1,0:T(2,128)(2,1)} %all-to-all-done.2) | data formatting | bytes 1048576
  163.6 4.4 %reshape.195 = bf16[128,1,1,2048]{3,2,1,0:T(2,128)(2,1)} reshape(bf16[128,2,1024]{2,1,0:T(2,128)(2,1)} %copy-done.2) | data formatting | bytes 1048576
  168.0 3.8 %all-to-all-done.4 = bf16[128,4,352]{2,1,0:T(4,128)(2,1)} async-done(((bf16[128,4,352]{2,1,0:T(4,128)(2,1)}), bf16[128,4,352]{2,1,0:T(4,128)(2,1)}, u32[]{:S(2)}, u32[]{:S(2)}) %all-to-all-start.4) | async-done | bytes 360480 | tf_op jit(solution)/shard_map/all_to_all | solution.py:183
  171.8 1.3 convolution_convert_fusion.4
  174.1 6.1 %all-to-all-start.5 = ((bf16[128,4,256]{2,1,0:T(4,128)(2,1)}), bf16[128,4,256]{2,1,0:T(4,128)(2,1)S(1)}, u32[]{:S(2)}, u32[]{:S(2)}) async-start(bf16[128,4,256]{2,1,0:T(4,128)(2,1)} %copy.89), calls=%async_computation.5 | async-start | bytes 524288 | tf_op jit(solution)/shard_map/all_to_all | solution.py:187
  180.1 3.5 %pad_maximum_fusion = bf16[128,1,2,2048]{3,2,1,0:T(2,128)(2,1)S(1)} fusion(bf16[128,1,1,2048]{3,2,1,0:T(2,128)(2,1)S(1)} %reshape.193, bf16[128,1,1,2048]{3,2,1,0:T(2,128)(2,1)} %reshape.195), kind=kLoop, calls=%fused_computation.30 | loop fusion | flops 2097152 | bytes 2097152 | tf_op jit(solution)/shard_map/concatenate | solution.py:44
  184.5 6.8 %all-to-all-done.5 = bf16[128,4,256]{2,1,0:T(4,128)(2,1)S(1)} async-done(((bf16[128,4,256]{2,1,0:T(4,128)(2,1)}), bf16[128,4,256]{2,1,0:T(4,128)(2,1)S(1)}, u32[]{:S(2)}, u32[]{:S(2)}) %all-to-all-start.5) | async-done | bytes 262176 | tf_op jit(solution)/shard_map/all_to_all | solution.py:187
  (91 shorter events, 13.9 us)
Async XLA Ops:
  7.2 15.6 %copy-start = (bf16[4,1024,2,128]{3,2,1,0:T(2,128)(2,1)S(1)}, bf16[4,1024,2,128]{3,2,1,0:T(2,128)(2,1)}, u32[]{:S(2)}) copy-start(bf16[4,1024,2,128]{3,2,1,0:T(2,128)(2,1)} %param.24) | copy-start | bytes 6291460
  7.2 97.9 %all-gather.3.cloned.1.call-start = ((), (), s32[]{:S(2)}) async-start(), calls=%async_computation.6 | async-start | bytes 2113536 | tf_op jit(solution)/shard_map/all_gather | solution.py:158
  8.2 2.9 %copy-start.17 = (s32[4]{0:T(128)S(1)}, s32[4]{0:T(128)}, u32[]{:S(2)}) copy-start(s32[4]{0:T(128)} %param.22) | copy-start | bytes 52
  11.3 6.8 %copy-start.4 = (bf16[2048,256]{1,0:T(8,128)(2,1)S(1)}, bf16[2048,256]{1,0:T(8,128)(2,1)}, u32[]{:S(2)}) copy-start(bf16[2048,256]{1,0:T(8,128)(2,1)} %param.26) | copy-start | bytes 3145732
  11.3 6.8 %copy-start.6 = (bf16[4,2048]{1,0:T(4,128)(2,1)S(1)}, bf16[4,2048]{1,0:T(4,128)(2,1)}, u32[]{:S(2)}) copy-start(bf16[4,2048]{1,0:T(4,128)(2,1)} %param.21) | copy-start | bytes 49156
  11.3 6.8 %copy-start.9 = (f32[2048]{0:T(1024)S(1)}, f32[2048]{0:T(1024)}, u32[]{:S(2)}) copy-start(f32[2048]{0:T(1024)} %param.31) | copy-start | bytes 24580
  11.3 7.5 %copy-start.18 = (f32[8]{0:T(128)S(1)}, f32[8]{0:T(128)}, u32[]{:S(2)}) copy-start(f32[8]{0:T(128)} %param.29) | copy-start | bytes 100
  11.3 7.6 %copy-start.5 = (bf16[2048,256]{1,0:T(8,128)(2,1)S(1)}, bf16[2048,256]{1,0:T(8,128)(2,1)}, u32[]{:S(2)}) copy-start(bf16[2048,256]{1,0:T(8,128)(2,1)} %param.27) | copy-start | bytes 3145732
  18.4 4.1 %copy-start.12 = (bf16[4,256]{1,0:T(4,128)(2,1)}, bf16[4,256]{1,0:T(4,128)(2,1)S(1)}, u32[]{:S(2)}) copy-start(bf16[4,256]{1,0:T(4,128)(2,1)S(1)} %convolution_convert_fusion.7) | copy-start | bytes 6148
  19.1 3.3 %copy-start.11 = (bf16[4,256]{1,0:T(4,128)(2,1)}, bf16[4,256]{1,0:T(4,128)(2,1)S(1)}, u32[]{:S(2)}) copy-start(bf16[4,256]{1,0:T(4,128)(2,1)S(1)} %convolution_convert_fusion.6) | copy-start | bytes 6148
  19.2 2.5 %copy-start.3 = (bf16[4,1024,2,64]{3,2,1,0:T(2,128)(2,1)S(1)}, bf16[4,1024,2,64]{3,2,1,0:T(2,128)(2,1)}, u32[]{:S(2)}) copy-start(bf16[4,1024,2,64]{3,2,1,0:T(2,128)(2,1)} %get-tuple-element.5) | copy-start | bytes 3145732
  22.7 0.7 copy-start.16
  23.5 3.0 %copy-start.10 = (f32[2048]{0:T(1024)S(1)}, f32[2048]{0:T(1024)}, u32[]{:S(2)}) copy-start(f32[2048]{0:T(1024)} %param.32) | copy-start | bytes 24580
  23.5 3.7 %copy-start.14 = (s32[4,2]{0,1:T(2,128)S(1)}, s32[4,2]{0,1:T(2,128)}, u32[]{:S(2)}) copy-start(s32[4,2]{0,1:T(2,128)} %param.33) | copy-start | bytes 100
  29.3 31.0 %all-to-all-start = ((bf16[128,2,2048]{2,1,0:T(2,128)(2,1)}), bf16[128,2,2048]{2,1,0:T(2,128)(2,1)}, u32[]{:S(2)}, u32[]{:S(2)}) async-start(bf16[128,2,2048]{2,1,0:T(2,128)(2,1)} %bitcast.7), calls=%async_computation | async-start | bytes 2097152 | tf_op jit(solution)/shard_map/all_to_all | solution.py:206
  79.8 34.3 %all-to-all-start.2 = ((bf16[128,2,1024]{2,1,0:T(2,128)(2,1)}), bf16[128,2,1024]{2,1,0:T(2,128)(2,1)}, u32[]{:S(2)}, u32[]{:S(2)}) async-start(bf16[128,2,1024]{2,1,0:T(2,128)(2,1)} %reshape.192), calls=%async_computation.2 | async-start | bytes 1048576 | tf_op jit(solution)/shard_map/all_to_all | solution.py:43
  85.2 24.9 %copy-start.7 = (bf16[1,256,352]{1,2,0:T(8,128)(2,1)S(1)}, bf16[1,256,352]{1,2,0:T(8,128)(2,1)}, u32[]{:S(2)}) copy-start(bf16[1,256,352]{1,2,0:T(8,128)(2,1)} %param.39) | copy-start | bytes 540676
  85.2 25.2 %copy-start.8 = (bf16[1,256,352]{1,2,0:T(8,128)(2,1)S(1)}, bf16[1,256,352]{1,2,0:T(8,128)(2,1)}, u32[]{:S(2)}) copy-start(bf16[1,256,352]{1,2,0:T(8,128)(2,1)} %param.38) | copy-start | bytes 540676
  110.7 9.5 %copy-start.1 = (bf16[128,1,1,2048]{3,2,1,0:T(2,128)(2,1)S(1)}, bf16[128,1,1,2048]{3,2,1,0:T(2,128)(2,1)}, u32[]{:S(2)}) copy-start(bf16[128,1,1,2048]{3,2,1,0:T(2,128)(2,1)} %get-tuple-element.7) | copy-start | bytes 1572868
  114.1 22.2 %all-to-all-start.3 = ((bf16[128,8,352]{2,1,0:T(8,128)(2,1)}), bf16[128,8,352]{2,1,0:T(8,128)(2,1)}, u32[]{:S(2)}, u32[]{:S(2)}) async-start(bf16[128,8,352]{2,1,0:T(8,128)(2,1)} %copy.84), calls=%async_computation.3 | async-start | bytes 1572864 | tf_op jit(solution)/shard_map/all_to_all | solution.py:17
  136.3 18.1 %all-to-all-start.1 = ((bf16[128,2,1024]{2,1,0:T(2,128)(2,1)}), bf16[128,2,1024]{2,1,0:T(2,128)(2,1)S(1)}, u32[]{:S(2)}, u32[]{:S(2)}) async-start(bf16[128,2,1024]{2,1,0:T(2,128)(2,1)} %reshape.194), calls=%async_computation.1 | async-start | bytes 1048576 | tf_op jit(solution)/shard_map/all_to_all | solution.py:43
  142.6 17.2 %copy-start.13 = (bf16[2048]{0:T(1024)(128)(2,1)S(1)}, bf16[2048]{0:T(1024)(128)(2,1)}, u32[]{:S(2)}) copy-start(bf16[2048]{0:T(1024)(128)(2,1)} %param.41) | copy-start | bytes 12292
  142.6 17.2 %copy-start.15 = (f32[4,2]{0,1:T(2,128)S(1)}, f32[4,2]{0,1:T(2,128)}, u32[]{:S(2)}) copy-start(f32[4,2]{0,1:T(2,128)} %param.34) | copy-start | bytes 100
  154.4 5.5 %copy-start.2 = (bf16[128,2,1024]{2,1,0:T(2,128)(2,1)}, bf16[128,2,1024]{2,1,0:T(2,128)(2,1)S(1)}, u32[]{:S(2)}) copy-start(bf16[128,2,1024]{2,1,0:T(2,128)(2,1)S(1)} %all-to-all-done.1) | copy-start | bytes 1572868
  154.4 17.4 %all-to-all-start.4 = ((bf16[128,4,352]{2,1,0:T(4,128)(2,1)}), bf16[128,4,352]{2,1,0:T(4,128)(2,1)}, u32[]{:S(2)}, u32[]{:S(2)}) async-start(bf16[128,4,352]{2,1,0:T(4,128)(2,1)} %copy.87), calls=%async_computation.4 | async-start | bytes 786432 | tf_op jit(solution)/shard_map/all_to_all | solution.py:183
  174.1 17.1 %all-to-all-start.5 = ((bf16[128,4,256]{2,1,0:T(4,128)(2,1)}), bf16[128,4,256]{2,1,0:T(4,128)(2,1)S(1)}, u32[]{:S(2)}, u32[]{:S(2)}) async-start(bf16[128,4,256]{2,1,0:T(4,128)(2,1)} %copy.89), calls=%async_computation.5 | async-start | bytes 524288 | tf_op jit(solution)/shard_map/all_to_all | solution.py:187
Sparse Core Ops, SparseCore 0:
  27.3 77.6 all-gather.2
where the time goes:
time: 200 us; the launch traced here: 199 us
  waiting for transfers between devices  69.5 us (35%)
  starting transfers between devices  39.4 us (20%)
  local copies, waits for them, and re-layouts  37.7 us (19%)
  matrix products  21 us (10%)
  other arithmetic  17 us (8%)
  between operations  14.5 us (7%)
    all_gather x1, waiting for transfers between devices, per_device(): all_rows = lax.all_gather(ffn_in, 'ep', axis=0, tiled=True)  19.9 us
    all_to_all x1, waiting for transfers between devices, per_device(): lax.all_to_all(outgoing, 'ep', split_axis=0, concat_axis=0, tiled=True)  19 us
    unnamed x46, local copies, waits for them, and re-layouts  15.6 us
    all_to_all x1, starting transfers between devices, per_device(): lax.all_to_all(outgoing, 'ep', split_axis=0, concat_axis=0, tiled=True)  12 us
    all_to_all x2, waiting for transfers between devices, exchange_in_pieces(): lax.all_to_all(piece, axis, split_axis=0, concat_axis=0, tiled=True)  10.5 us
    all_to_all x2, starting transfers between devices, exchange_in_pieces(): lax.all_to_all(piece, axis, split_axis=0, concat_axis=0, tiled=True)  9.93 us
    all_to_all x1, waiting for transfers between devices, sent_together(): lax.all_to_all(both, axis, split_axis=split_dim, concat_axis=concat_dim,...  9.43 us
    split x2, other arithmetic, exchange_in_pieces(): jnp.split(tiles, cut_rows(tiles.shape[cut], pieces), axis=cut)  9.13 us
  transfers between devices with their start and end apart: 7, of which 6 were waited for; matrix products, arithmetic and copies ran while one was open for 26% of the time, Pallas kernels for 0%

commit v1 on v0

--- a/solution.py
+++ b/solution.py
@@ -155,7 +155,10 @@
     row_blocks = devices // SPLIT
     capacity = min(SEQ_DEV, max(2, SEQ_DEV * TOP_K * 2 // experts))
     slots = jnp.arange(capacity, dtype=jnp.int32)
-    all_rows = lax.all_gather(ffn_in, "ep", axis=0, tiled=True)
+    size = lax.axis_size("ep")
+    blocks = jnp.stack([ffn_in for _ in range(size)])
+    blocks = lax.all_to_all(blocks, "ep", split_axis=0, concat_axis=0)
+    all_rows = jnp.concatenate(blocks, axis=0)
     gate = jax.nn.sigmoid(jnp.dot(ffn_in, branch_gate, preferred_element_type=jnp.float32))
     position = lax.axis_index("ep")
     row_span = dense_gate.shape[1]

time: 200 us -> 188 us (0.940)
  blocking collectives: 0 us -> 30.6 us
  waiting for transfers between devices: 69.5 us -> 45.7 us
  between operations: 14.5 us -> 1.2 us
  starting transfers between devices: 39.4 us -> 32.8 us
    all_to_all x0 -> x1, blocking collectives: none -> 30.6 us  [per_device(): lax.all_to_all(outgoing, 'ep', split_axis=0, concat_axis=0, tiled=True)]
    all_gather x1 -> x0, waiting for transfers between devices: 19.9 us -> none  [per_device(): all_rows = lax.all_gather(ffn_in, 'ep', axis=0, tiled=True)]
    all_to_all x1, waiting for transfers between devices: 19 us -> 11.8 us  [per_device(): blocks = lax.all_to_all(blocks, 'ep', split_axis=0, concat_axis=0)]
    all_to_all x1, starting transfers between devices: 12 us -> 5.49 us  [per_device(): blocks = lax.all_to_all(blocks, 'ep', split_axis=0, concat_axis=0)]
    all_to_all x2, waiting for transfers between devices: 10.5 us -> 14.8 us  [exchange_in_pieces(): lax.all_to_all(piece, axis, split_axis=0, concat_axis=0, tiled=True)]
    reshape x0 -> x1, local copies, waits for them, and re-layouts: none -> 3.99 us  [per_device(): all_rows = jnp.concatenate(blocks, axis=0)]
    unnamed x46 -> x63, local copies, waits for them, and re-layouts: 15.6 us -> 11.9 us
    another operation x0 -> x1, local copies, waits for them, and re-layouts: none -> 2.36 us  [per_device(): blocks = jnp.stack([ffn_in for _ in range(size)])]
  transfers between devices with their start and end apart: 7 -> 6, of which waited for: 6 -> 6; matrix products, arithmetic and copies ran while one was open for 26% -> 27% of each run, Pallas kernels for 0% -> 0%
where the time goes in v1:
time: 188 us; the launch traced here: 187 us
  waiting for transfers between devices  45.7 us (24%)
  local copies, waits for them, and re-layouts  39.2 us (21%)
  starting transfers between devices  32.8 us (17%)
  blocking collectives  30.6 us (16%)
  matrix products  20.4 us (11%)
  other arithmetic  17.1 us (9%)
    all_to_all x1, blocking collectives, per_device(): lax.all_to_all(outgoing, 'ep', split_axis=0, concat_axis=0, tiled=True)  30.6 us
    all_to_all x2, waiting for transfers between devices, exchange_in_pieces(): lax.all_to_all(piece, axis, split_axis=0, concat_axis=0, tiled=True)  14.8 us
    unnamed x63, local copies, waits for them, and re-layouts  11.9 us
    all_to_all x1, waiting for transfers between devices, per_device(): blocks = lax.all_to_all(blocks, 'ep', split_axis=0, concat_axis=0)  11.8 us
    all_to_all x2, starting transfers between devices, exchange_in_pieces(): lax.all_to_all(piece, axis, split_axis=0, concat_axis=0, tiled=True)  9.93 us
    all_to_all x1, waiting for transfers between devices, sent_together(): lax.all_to_all(both, axis, split_axis=split_dim, concat_axis=concat_dim,...  9.39 us
    split x2, other arithmetic, exchange_in_pieces(): jnp.split(tiles, cut_rows(tiles.shape[cut], pieces), axis=cut)  9.27 us
    all_to_all x1, starting transfers between devices, per_device(): lax.all_to_all(down_tile.reshape(devices, rows, row_span).astype(jnp.bflo...  6.81 us
  transfers between devices with their start and end apart: 6, of which 6 were waited for; matrix products, arithmetic and copies ran while one was open for 27% of the time, Pallas kernels for 0%

profile of v1, /device:TPU:1, one launch (start us, length us, event | category | flops | bytes accessed | tf_op | source)
XLA Modules:
  0.0 187.0 jit_solution(664203328900374658)
XLA Ops:
  1.7 2.9 %convolution_convert_fusion.5 = bf16[4,1024]{1,0:T(4,128)(2,1)S(1)} fusion(bf16[2048,1024]{1,0:T(8,128)(2,1)} %param.25, bf16[4,2048]{1,0:T(4,128)(2,1)} %param.21, f32[2048]{0:T(1024)} %param.31, f32[4]{0:T(128)S(1)} %add_rsqrt_fusion.2), kind=kOutput, calls=%fused_computation.22 | convolution fusion | flops 16814080 | bytes 4227088 | tf_op jit(solution)/shard_map/dot_general | solution.py:98
  4.7 6.7 %fusion.79 = (bf16[4,1024,2,64]{3,2,1,0:T(2,128)(2,1)}, bf16[4,1024,2,64]{3,2,1,0:T(2,128)(2,1)}) fusion(bf16[4,1024,2,128]{3,2,1,0:T(2,128)(2,1)} %param.23), kind=kLoop, calls=%fused_computation.114 | loop fusion | bytes 4194304 | tf_op jit(solution)/shard_map/slice | solution.py:127
  12.9 2.5 %select_reduce_fusion.1 = (f32[4,2,4]{2,1,0:T(2,128)S(1)}, f32[4,2,4,1024]{3,2,1,0:T(4,128)S(1)}) fusion(pred[4,1024]{1,0:T(4,128)(4,1)S(1)} %iota_compare_fusion, bf16[4,1024,2,64]{3,2,1,0:T(2,128)(2,1)} %get-tuple-element.6, bf16[4,2,4,128]{3,2,1,0:T(4,128)(2,1)S(1)} %reshape.164), kind=kOutput, calls=%fused_computation.52 | convolution fusion | flops 4292576 | bytes 1192064 | tf_op jit(solution)/shard_map/sgqd,spgd->sgqp/dot_general | solution.py:106
  17.2 3.0 %multiply_reduce_fusion = (f32[4]{0:T(128)S(1)}, f32[4,2048]{1,0:T(4,128)S(1)}) fusion(bf16[4,1024]{1,0:T(4,128)(2,1)S(1)} %reshape.166, bf16[1024,2048]{1,0:T(8,128)(2,1)} %param.28, bf16[4,2048]{1,0:T(4,128)(2,1)S(1)} %copy-done.6), kind=kOutput, calls=%fused_computation.70 | convolution fusion | flops 16809980 | bytes 4251664 | tf_op jit(solution)/shard_map/dot_general | solution.py:151
  21.4 30.6 %all_to_all.35 = bf16[128,2,2048]{2,1,0:T(2,128)(2,1)} all-to-all(bf16[128,2,2048]{2,1,0:T(2,128)(2,1)S(1)} %bitcast.73), channel_id=1, replica_groups=mesh['ep'=128] {'ep'}, dimensions={0} | all-to-all | bytes 2097152 | tf_op jit(solution)/shard_map/all_to_all | solution.py:209
  52.0 2.4 %stack.2 = bf16[128,4,2048]{2,1,0:T(4,128)(2,1)} broadcast(bf16[4,2048]{1,0:T(4,128)(2,1)S(1)} %multiply_convert_fusion.1), dimensions={1,2} | broadcast | bytes 2113536 | tf_op jit(solution)/shard_map/stack | solution.py:159
  54.4 5.5 %all-to-all-start.3 = ((bf16[128,4,2048]{2,1,0:T(4,128)(2,1)}), bf16[128,4,2048]{2,1,0:T(4,128)(2,1)}, u32[]{:S(2)}, u32[]{:S(2)}) async-start(bf16[128,4,2048]{2,1,0:T(4,128)(2,1)} %stack.2), calls=%async_computation.3 | async-start | bytes 4194304 | tf_op jit(solution)/shard_map/all_to_all | solution.py:160
  59.9 1.5 reshape.168
  61.4 2.1 %fusion.82 = f32[256,384]{1,0:T(8,128)S(1)} fusion(bf16[256,2048]{1,0:T(8,128)(2,1)S(1)} %reshape.168, bf16[2048,384]{1,0:T(8,128)(2,1)} %param.35), kind=kOutput, calls=%fused_computation.117 | convolution fusion | flops 402653184 | bytes 3014656 | tf_op jit(solution)/shard_map/dot_general | solution.py:62
  63.5 4.2 %convolution_convert_fusion = bf16[256,2048]{1,0:T(8,128)(2,1)} fusion(bf16[384,2048]{1,0:T(8,128)(2,1)} %param.37, bf16[256,2048]{1,0:T(8,128)(2,1)S(1)} %reshape.168, bf16[2048,384]{1,0:T(8,128)(2,1)} %param.36, f32[256,384]{1,0:T(8,128)S(1)} %fusion.82), kind=kOutput, calls=%fused_computation | convolution fusion | flops 806420480 | bytes 5636096 | tf_op jit(solution)/shard_map/dot_general | solution.py:65
  67.7 1.7 convert_element_type.121
  69.4 2.5 %fusion.80 = (bf16[128,1,1,2048]{3,2,1,0:T(2,128)(2,1)}, bf16[128,1,1,2048]{3,2,1,0:T(2,128)(2,1)}) fusion(bf16[128,1,2,2048]{3,2,1,0:T(2,128)(2,1)S(1)} %bitcast.71), kind=kLoop, calls=%fused_computation.115 | loop fusion | bytes 2097152 | tf_op jit(solution)/shard_map/split | solution.py:41
  72.4 4.8 %reduce = bf16[128,2048]{1,0:T(8,128)(2,1)S(1)} reduce(bf16[128,1,1,2048]{3,2,1,0:T(2,128)(2,1)} %get-tuple-element.8, bf16[]{:T(256)} %broadcast.144), dimensions={1,2}, to_apply=%get-tuple-element.8.reduce_sub_computation | reduce | bytes 1048578 | tf_op jit(solution)/shard_map/split | solution.py:41
  78.3 11.8 %all-to-all-done.3 = bf16[128,4,2048]{2,1,0:T(4,128)(2,1)} async-done(((bf16[128,4,2048]{2,1,0:T(4,128)(2,1)}), bf16[128,4,2048]{2,1,0:T(4,128)(2,1)}, u32[]{:S(2)}, u32[]{:S(2)}) %all-to-all-start.3) | async-done | bytes 2097184 | tf_op jit(solution)/shard_map/all_to_all | solution.py:160
  90.1 5.4 %all-to-all-start.2 = ((bf16[128,2,1024]{2,1,0:T(2,128)(2,1)}), bf16[128,2,1024]{2,1,0:T(2,128)(2,1)}, u32[]{:S(2)}, u32[]{:S(2)}) async-start(bf16[128,2,1024]{2,1,0:T(2,128)(2,1)} %reshape.196), calls=%async_computation.2 | async-start | bytes 1048576 | tf_op jit(solution)/shard_map/all_to_all | solution.py:43
  95.6 4.0 %reshape.169 = bf16[512,2048]{1,0:T(8,128)(2,1)} reshape(bf16[128,4,2048]{2,1,0:T(4,128)(2,1)} %all-to-all-done.3) | data formatting | bytes 4194304 | tf_op jit(solution)/shard_map/reshape | solution.py:161
  102.2 2.4 %copy.84 = bf16[128,8,352]{2,1,0:T(8,128)(2,1)} copy(bf16[128,8,352]{0,2,1:T(8,128)(2,1)} %pad_maximum_fusion.1) | data formatting | bytes 1441792 | tf_op jit(solution)/shard_map/concatenate | solution.py:16
  104.6 4.3 %all-to-all-done.2 = bf16[128,2,1024]{2,1,0:T(2,128)(2,1)} async-done(((bf16[128,2,1024]{2,1,0:T(2,128)(2,1)}), bf16[128,2,1024]{2,1,0:T(2,128)(2,1)}, u32[]{:S(2)}, u32[]{:S(2)}) %all-to-all-start.2) | async-done | bytes 524320 | tf_op jit(solution)/shard_map/all_to_all | solution.py:43
  108.9 6.0 %all-to-all-start.4 = ((bf16[128,8,352]{2,1,0:T(8,128)(2,1)}), bf16[128,8,352]{2,1,0:T(8,128)(2,1)}, u32[]{:S(2)}, u32[]{:S(2)}) async-start(bf16[128,8,352]{2,1,0:T(8,128)(2,1)} %copy.84), calls=%async_computation.4 | async-start | bytes 1572864 | tf_op jit(solution)/shard_map/all_to_all | solution.py:17
  114.9 4.5 %reduce.1 = bf16[128,2048]{1,0:T(8,128)(2,1)} reduce(bf16[128,1,1,2048]{3,2,1,0:T(2,128)(2,1)S(1)} %copy-done.1, bf16[]{:T(256)} %broadcast.144), dimensions={1,2}, to_apply=%get-tuple-element.7.reduce_sub_computation | reduce | bytes 1048578 | tf_op jit(solution)/shard_map/split | solution.py:41
  119.4 2.2 %reshape.198 = bf16[128,2,1024]{2,1,0:T(2,128)(2,1)} reshape(bf16[128,2048]{1,0:T(8,128)(2,1)} %reduce.1) | data formatting | bytes 1048576
  121.7 9.4 %all-to-all-done.4 = bf16[128,8,352]{2,1,0:T(8,128)(2,1)} async-done(((bf16[128,8,352]{2,1,0:T(8,128)(2,1)}), bf16[128,8,352]{2,1,0:T(8,128)(2,1)}, u32[]{:S(2)}, u32[]{:S(2)}) %all-to-all-start.4) | async-done | bytes 720928 | tf_op jit(solution)/shard_map/all_to_all | solution.py:17
  131.0 4.5 %all-to-all-start.1 = ((bf16[128,2,1024]{2,1,0:T(2,128)(2,1)}), bf16[128,2,1024]{2,1,0:T(2,128)(2,1)S(1)}, u32[]{:S(2)}, u32[]{:S(2)}) async-start(bf16[128,2,1024]{2,1,0:T(2,128)(2,1)} %reshape.198), calls=%async_computation.1 | async-start | bytes 1048576 | tf_op jit(solution)/shard_map/all_to_all | solution.py:43
  135.6 1.7 fusion.81
  138.7 10.5 %all-to-all-done.1 = bf16[128,2,1024]{2,1,0:T(2,128)(2,1)S(1)} async-done(((bf16[128,2,1024]{2,1,0:T(2,128)(2,1)}), bf16[128,2,1024]{2,1,0:T(2,128)(2,1)S(1)}, u32[]{:S(2)}, u32[]{:S(2)}) %all-to-all-start.1) | async-done | bytes 524320 | tf_op jit(solution)/shard_map/all_to_all | solution.py:43
  149.2 4.6 %all-to-all-start.5 = ((bf16[128,4,352]{2,1,0:T(4,128)(2,1)}), bf16[128,4,352]{2,1,0:T(4,128)(2,1)S(1)}, u32[]{:S(2)}, u32[]{:S(2)}) async-start(bf16[128,4,352]{2,1,0:T(4,128)(2,1)} %copy.87), calls=%async_computation.5 | async-start | bytes 786432 | tf_op jit(solution)/shard_map/all_to_all | solution.py:186
  155.1 3.6 %reshape.197 = bf16[128,1,1,2048]{3,2,1,0:T(2,128)(2,1)S(1)} reshape(bf16[128,2,1024]{2,1,0:T(2,128)(2,1)} %all-to-all-done.2) | data formatting | bytes 1048576
  158.7 4.3 %reshape.199 = bf16[128,1,1,2048]{3,2,1,0:T(2,128)(2,1)} reshape(bf16[128,2,1024]{2,1,0:T(2,128)(2,1)} %copy-done.2) | data formatting | bytes 1048576
  163.0 3.0 %all-to-all-done.5 = bf16[128,4,352]{2,1,0:T(4,128)(2,1)S(1)} async-done(((bf16[128,4,352]{2,1,0:T(4,128)(2,1)}), bf16[128,4,352]{2,1,0:T(4,128)(2,1)S(1)}, u32[]{:S(2)}, u32[]{:S(2)}) %all-to-all-start.5) | async-done | bytes 360480 | tf_op jit(solution)/shard_map/all_to_all | solution.py:186
  168.1 6.8 %all-to-all-start.6 = ((bf16[128,4,256]{2,1,0:T(4,128)(2,1)}), bf16[128,4,256]{2,1,0:T(4,128)(2,1)S(1)}, u32[]{:S(2)}, u32[]{:S(2)}) async-start(bf16[128,4,256]{2,1,0:T(4,128)(2,1)} %copy.89), calls=%async_computation.6 | async-start | bytes 524288 | tf_op jit(solution)/shard_map/all_to_all | solution.py:190
  175.0 3.5 %pad_maximum_fusion = bf16[128,1,2,2048]{3,2,1,0:T(2,128)(2,1)S(1)} fusion(bf16[128,1,1,2048]{3,2,1,0:T(2,128)(2,1)S(1)} %reshape.197, bf16[128,1,1,2048]{3,2,1,0:T(2,128)(2,1)} %reshape.199), kind=kLoop, calls=%fused_computation.30 | loop fusion | flops 2097152 | bytes 2097152 | tf_op jit(solution)/shard_map/concatenate | solution.py:44
  179.3 6.7 %all-to-all-done.6 = bf16[128,4,256]{2,1,0:T(4,128)(2,1)S(1)} async-done(((bf16[128,4,256]{2,1,0:T(4,128)(2,1)}), bf16[128,4,256]{2,1,0:T(4,128)(2,1)S(1)}, u32[]{:S(2)}, u32[]{:S(2)}) %all-to-all-start.6) | async-done | bytes 262176 | tf_op jit(solution)/shard_map/all_to_all | solution.py:190
  (107 shorter events, 16.4 us)
Async XLA Ops:
  0.6 15.8 %copy-start = (bf16[4,1024,2,128]{3,2,1,0:T(2,128)(2,1)S(1)}, bf16[4,1024,2,128]{3,2,1,0:T(2,128)(2,1)}, u32[]{:S(2)}) copy-start(bf16[4,1024,2,128]{3,2,1,0:T(2,128)(2,1)} %param.24) | copy-start | bytes 6291460
  1.7 2.9 %copy-start.26 = (s32[4]{0:T(128)S(1)}, s32[4]{0:T(128)}, u32[]{:S(2)}) copy-start(s32[4]{0:T(128)} %param.22) | copy-start | bytes 52
  4.7 6.8 %copy-start.4 = (bf16[2048,256]{1,0:T(8,128)(2,1)S(1)}, bf16[2048,256]{1,0:T(8,128)(2,1)}, u32[]{:S(2)}) copy-start(bf16[2048,256]{1,0:T(8,128)(2,1)} %param.26) | copy-start | bytes 3145732
  4.7 6.8 %copy-start.6 = (bf16[4,2048]{1,0:T(4,128)(2,1)S(1)}, bf16[4,2048]{1,0:T(4,128)(2,1)}, u32[]{:S(2)}) copy-start(bf16[4,2048]{1,0:T(4,128)(2,1)} %param.21) | copy-start | bytes 49156
  4.7 6.8 %copy-start.11 = (f32[2048]{0:T(1024)S(1)}, f32[2048]{0:T(1024)}, u32[]{:S(2)}) copy-start(f32[2048]{0:T(1024)} %param.31) | copy-start | bytes 24580
  4.7 7.8 %copy-start.27 = (f32[8]{0:T(128)S(1)}, f32[8]{0:T(128)}, u32[]{:S(2)}) copy-start(f32[8]{0:T(128)} %param.29) | copy-start | bytes 100
  4.7 7.9 %copy-start.5 = (bf16[2048,256]{1,0:T(8,128)(2,1)S(1)}, bf16[2048,256]{1,0:T(8,128)(2,1)}, u32[]{:S(2)}) copy-start(bf16[2048,256]{1,0:T(8,128)(2,1)} %param.27) | copy-start | bytes 3145732
  12.9 3.3 %copy-start.14 = (bf16[4,256]{1,0:T(4,128)(2,1)}, bf16[4,256]{1,0:T(4,128)(2,1)S(1)}, u32[]{:S(2)}) copy-start(bf16[4,256]{1,0:T(4,128)(2,1)S(1)} %convolution_convert_fusion.6) | copy-start | bytes 6148
  12.9 2.5 %copy-start.3 = (bf16[4,1024,2,64]{3,2,1,0:T(2,128)(2,1)S(1)}, bf16[4,1024,2,64]{3,2,1,0:T(2,128)(2,1)}, u32[]{:S(2)}) copy-start(bf16[4,1024,2,64]{3,2,1,0:T(2,128)(2,1)} %get-tuple-element.5) | copy-start | bytes 3145732
  17.2 3.0 %copy-start.21 = (s32[4,2]{0,1:T(2,128)S(1)}, s32[4,2]{0,1:T(2,128)}, u32[]{:S(2)}) copy-start(s32[4,2]{0,1:T(2,128)} %param.33) | copy-start | bytes 100
  17.2 3.2 %copy-start.17 = (f32[2048]{0:T(1024)S(1)}, f32[2048]{0:T(1024)}, u32[]{:S(2)}) copy-start(f32[2048]{0:T(1024)} %param.32) | copy-start | bytes 24580
  20.2 34.2 %copy-start.7 = (f32[4,2048]{1,0:T(4,128)}, f32[4,2048]{1,0:T(4,128)S(1)}, u32[]{:S(2)}) copy-start(f32[4,2048]{1,0:T(4,128)S(1)} %get-tuple-element.24) | copy-start | bytes 98308
  20.3 34.0 %copy-start.18 = (pred[8,4]{0,1:T(4,128)(4,1)}, pred[8,4]{0,1:T(4,128)(4,1)S(1)}, u32[]{:S(2)}) copy-start(pred[8,4]{0,1:T(4,128)(4,1)S(1)} %get-tuple-element.16) | copy-start | bytes 100
  20.4 34.0 %copy-start.12 = (s32[8,4]{0,1:T(4,128)}, s32[8,4]{0,1:T(4,128)S(1)}, u32[]{:S(2)}) copy-start(s32[8,4]{0,1:T(4,128)S(1)} %broadcast_add_fusion) | copy-start | bytes 388
  54.4 35.7 %all-to-all-start.3 = ((bf16[128,4,2048]{2,1,0:T(4,128)(2,1)}), bf16[128,4,2048]{2,1,0:T(4,128)(2,1)}, u32[]{:S(2)}, u32[]{:S(2)}) async-start(bf16[128,4,2048]{2,1,0:T(4,128)(2,1)} %stack.2), calls=%async_computation.3 | async-start | bytes 4194304 | tf_op jit(solution)/shard_map/all_to_all | solution.py:160
  90.1 18.8 %all-to-all-start.2 = ((bf16[128,2,1024]{2,1,0:T(2,128)(2,1)}), bf16[128,2,1024]{2,1,0:T(2,128)(2,1)}, u32[]{:S(2)}, u32[]{:S(2)}) async-start(bf16[128,2,1024]{2,1,0:T(2,128)(2,1)} %reshape.196), calls=%async_computation.2 | async-start | bytes 1048576 | tf_op jit(solution)/shard_map/all_to_all | solution.py:43
  95.5 5.1 %copy-start.9 = (bf16[1,256,352]{1,2,0:T(8,128)(2,1)S(1)}, bf16[1,256,352]{1,2,0:T(8,128)(2,1)}, u32[]{:S(2)}) copy-start(bf16[1,256,352]{1,2,0:T(8,128)(2,1)} %param.39) | copy-start | bytes 540676
  95.5 5.3 %copy-start.10 = (bf16[1,256,352]{1,2,0:T(8,128)(2,1)S(1)}, bf16[1,256,352]{1,2,0:T(8,128)(2,1)}, u32[]{:S(2)}) copy-start(bf16[1,256,352]{1,2,0:T(8,128)(2,1)} %param.38) | copy-start | bytes 540676
  101.2 13.7 %copy-start.1 = (bf16[128,1,1,2048]{3,2,1,0:T(2,128)(2,1)S(1)}, bf16[128,1,1,2048]{3,2,1,0:T(2,128)(2,1)}, u32[]{:S(2)}) copy-start(bf16[128,1,1,2048]{3,2,1,0:T(2,128)(2,1)} %get-tuple-element.7) | copy-start | bytes 1572868
  108.9 22.1 %all-to-all-start.4 = ((bf16[128,8,352]{2,1,0:T(8,128)(2,1)}), bf16[128,8,352]{2,1,0:T(8,128)(2,1)}, u32[]{:S(2)}, u32[]{:S(2)}) async-start(bf16[128,8,352]{2,1,0:T(8,128)(2,1)} %copy.84), calls=%async_computation.4 | async-start | bytes 1572864 | tf_op jit(solution)/shard_map/all_to_all | solution.py:17
  131.0 18.1 %all-to-all-start.1 = ((bf16[128,2,1024]{2,1,0:T(2,128)(2,1)}), bf16[128,2,1024]{2,1,0:T(2,128)(2,1)S(1)}, u32[]{:S(2)}, u32[]{:S(2)}) async-start(bf16[128,2,1024]{2,1,0:T(2,128)(2,1)} %reshape.198), calls=%async_computation.1 | async-start | bytes 1048576 | tf_op jit(solution)/shard_map/all_to_all | solution.py:43
  137.3 16.5 %copy-start.20 = (bf16[2048]{0:T(1024)(128)(2,1)S(1)}, bf16[2048]{0:T(1024)(128)(2,1)}, u32[]{:S(2)}) copy-start(bf16[2048]{0:T(1024)(128)(2,1)} %param.41) | copy-start | bytes 12292
  137.3 16.5 %copy-start.22 = (s32[4,2]{0,1:T(2,128)S(1)}, s32[4,2]{0,1:T(2,128)}, u32[]{:S(2)}) copy-start(s32[4,2]{0,1:T(2,128)} %param.33) | copy-start | bytes 100
  137.3 16.5 %copy-start.23 = (f32[4,2]{0,1:T(2,128)S(1)}, f32[4,2]{0,1:T(2,128)}, u32[]{:S(2)}) copy-start(f32[4,2]{0,1:T(2,128)} %param.34) | copy-start | bytes 100
  149.2 5.3 %copy-start.2 = (bf16[128,2,1024]{2,1,0:T(2,128)(2,1)}, bf16[128,2,1024]{2,1,0:T(2,128)(2,1)S(1)}, u32[]{:S(2)}) copy-start(bf16[128,2,1024]{2,1,0:T(2,128)(2,1)S(1)} %all-to-all-done.1) | copy-start | bytes 1572868
  149.2 16.8 %all-to-all-start.5 = ((bf16[128,4,352]{2,1,0:T(4,128)(2,1)}), bf16[128,4,352]{2,1,0:T(4,128)(2,1)S(1)}, u32[]{:S(2)}, u32[]{:S(2)}) async-start(bf16[128,4,352]{2,1,0:T(4,128)(2,1)} %copy.87), calls=%async_computation.5 | async-start | bytes 786432 | tf_op jit(solution)/shard_map/all_to_all | solution.py:186
  168.1 17.9 %all-to-all-start.6 = ((bf16[128,4,256]{2,1,0:T(4,128)(2,1)}), bf16[128,4,256]{2,1,0:T(4,128)(2,1)S(1)}, u32[]{:S(2)}, u32[]{:S(2)}) async-start(bf16[128,4,256]{2,1,0:T(4,128)(2,1)} %copy.89), calls=%async_computation.6 | async-start | bytes 524288 | tf_op jit(solution)/shard_map/all_to_all | solution.py:190
  174.9 11.2 %copy-start.8 = (f32[4,2048]{1,0:T(4,128)S(1)}, f32[4,2048]{1,0:T(4,128)}, u32[]{:S(2)}) copy-start(f32[4,2048]{1,0:T(4,128)} %copy-done.7) | copy-start | bytes 98308
  174.9 11.2 %copy-start.13 = (s32[8,4]{0,1:T(4,128)S(1)}, s32[8,4]{0,1:T(4,128)}, u32[]{:S(2)}) copy-start(s32[8,4]{0,1:T(4,128)} %copy-done.12) | copy-start | bytes 388
  175.0 11.2 %copy-start.16 = (f32[8,4]{0,1:T(4,128)S(1)}, f32[8,4]{0,1:T(4,128)}, u32[]{:S(2)}) copy-start(f32[8,4]{0,1:T(4,128)} %select_reduce_fusion.2) | copy-start | bytes 388
  175.0 11.2 %copy-start.19 = (pred[8,4]{0,1:T(4,128)(4,1)S(1)}, pred[8,4]{0,1:T(4,128)(4,1)}, u32[]{:S(2)}) copy-start(pred[8,4]{0,1:T(4,128)(4,1)} %copy-done.18) | copy-start | bytes 100
  175.0 11.2 %copy-start.25 = (f32[4]{0:T(128)S(1)}, f32[4]{0:T(128)}, u32[]{:S(2)}) copy-start(f32[4]{0:T(128)} %fusion.22) | copy-start | bytes 52
  (2 other events, 1.2 us)
